TPU v7x, 256 devices: a whole 4x4x8 slice. The times are simulated.
256 devices in a mesh: fs: 32 (over z, x), tp: 8 (over y, core).
Axes of the slice: x: 4, y: 4, z: 8, core: 2. Of those that a mesh axis runs over, the one named last changes fastest.
Arguments:
- tokens: bfloat16 [32768, 2048], P(('fs', 'tp')), may hold values from -6 to 6
- gate_pre: bfloat16 [32768, 5632], P('fs', 'tp'), may hold values from -6 to 6
- value_pre: bfloat16 [32768, 5632], P('fs', 'tp'), may hold values from -6 to 6
- up_gate_w: bfloat16 [2048, 5632], P('fs', 'tp'), may hold values from -0.078125 to 0.078125
- up_value_w: bfloat16 [2048, 5632], P('fs', 'tp'), may hold values from -0.078125 to 0.078125
- conv_weight: float32 [3, 5632], P(None, 'tp'), may hold values from -3 to 3
- conv_bias: float32 [5632], P('tp'), may hold values from -3 to 3
- hidden_grad: bfloat16 [32768, 5632], P('fs', 'tp'), may hold values from -6 to 6
Outputs:
- input_grad: bfloat16 [32768, 2048], P(('fs', 'tp'))
- up_gate_grad: float32 [2048, 5632], P('fs', 'tp')
- up_value_grad: float32 [2048, 5632], P('fs', 'tp')
- conv_weight_grad: float32 [3, 5632], P(None, 'tp')
- conv_bias_grad: float32 [5632], P('tp')
All inputs are finite; a program needn't handle non-finite values.
Results may differ from a plain program's by a relative error of at most 0.013.
Values may be sent and summed in bfloat16 or wider, within the bound.
No kernel may reach another device: no remote copies, remote signals or barrier semaphores. Data moves between devices by JAX's collectives and lax.ppermute only.
A program may use at most 128 MiB of HBM per device.

v0:
```python
import jax
import jax.numpy as jnp
from jax import lax
from jax.sharding import Mesh
from jax.sharding import PartitionSpec as P

FS = ("fs_0", "fs_1")
FS_TP = ("fs_0", "fs_1", "tp")


def copy_for_each(shard, axis):
    peers = lax.axis_size(axis)
    return lax.all_to_all(
        jnp.broadcast_to(shard[None], (peers, *shard.shape)), axis, 0, 0, tiled=True
    )


def taken_together(shard, axis):
    return copy_for_each(shard, axis).sum(axis=0)


def in_one_piece(arrays, axis, dim, along):
    ends, at = ([], 0)
    for a in arrays[:-1]:
        at += a.shape[along]
        ends.append(at)
    both = jnp.concatenate(arrays, axis=along)
    return tuple(jnp.split(lax.all_gather(both, axis, axis=dim, tiled=True), ends, axis=along))


def summed_rows(subtotal, axes):
    return lax.psum_scatter(
        subtotal.astype(jnp.bfloat16), axes, scatter_dimension=0, tiled=True
    ).astype(jnp.float32)


def in_blocks(shard, dim, peers):
    lengths = shard.shape
    blocks = shard.reshape(*lengths[:dim], peers, lengths[dim] // peers, *lengths[dim + 1 :])
    return jnp.moveaxis(blocks, dim, 0)


def summed_on_arrival(shard, axis, dim):
    blocks = in_blocks(shard, dim, lax.axis_size(axis))
    arrived = lax.all_to_all(blocks, axis, split_axis=0, concat_axis=0, tiled=True)
    return arrived.astype(jnp.float32).sum(axis=0)


def contract_rows(left, right):
    return lax.dot_general(
        left, right, (((0,), (0,)), ((), ())), preferred_element_type=jnp.float32
    )


def contract_cols(left, right):
    return lax.dot_general(
        left, right, (((1,), (1,)), ((), ())), preferred_element_type=jnp.float32
    )


def on_device(
    tokens, gate_pre, value_pre, up_gate_w, up_value_w, conv_weight, conv_bias, hidden_grad
):
    length = gate_pre.shape[0]
    col_count = gate_pre.shape[1]
    scale = float(length * lax.axis_size(FS)) ** (-0.5)
    gate_float = gate_pre.astype(jnp.float32)
    padded = jnp.pad(gate_float, ((2, 0), (0, 0)))
    gate_conv = (
        conv_bias
        + conv_weight[0] * padded[:length]
        + conv_weight[1] * padded[1 : length + 1]
        + conv_weight[2] * padded[2:]
    )
    active, gelu_back = jax.vjp(jax.nn.gelu, gate_conv)
    grad_float = hidden_grad.astype(jnp.float32)
    value_grad = (grad_float * active).astype(jnp.bfloat16)
    conv_grad = gelu_back(grad_float * value_pre.astype(jnp.float32))[0]
    shifted = jnp.pad(conv_grad, ((0, 2), (0, 0)))
    gate_grad = (
        conv_weight[2] * conv_grad
        + conv_weight[1] * shifted[1 : length + 1]
        + conv_weight[0] * shifted[2:]
    ).astype(jnp.bfloat16)
    conv_terms = jnp.stack(
        [
            jnp.sum(conv_grad * padded[:length], axis=0),
            jnp.sum(conv_grad * padded[1 : length + 1], axis=0),
            jnp.sum(conv_grad * padded[2:], axis=0),
            jnp.sum(conv_grad, axis=0),
        ]
    )
    conv_total = taken_together(conv_terms, FS) * scale
    whole_tokens = lax.all_gather(tokens, "tp", axis=0, tiled=True)
    full_gate, full_value = in_one_piece((up_gate_w, up_value_w), FS, 0, 1)
    joined = summed_rows(
        jnp.concatenate(
            [contract_rows(whole_tokens, gate_grad), contract_rows(whole_tokens, value_grad)],
            axis=1,
        ),
        FS,
    )
    gate_out = joined[:, :col_count] * scale
    value_out = joined[:, col_count:] * scale
    input_grad = summed_on_arrival(
        (contract_cols(gate_grad, full_gate) + contract_cols(value_grad, full_value)).astype(
            jnp.bfloat16
        ),
        "tp",
        0,
    ).astype(jnp.bfloat16)
    return (input_grad, gate_out, value_out, conv_total[:3], conv_total[3])


def solution(mesh):
    finer = Mesh(mesh.devices.reshape(8, 4, mesh.shape["tp"]), ("fs_0", "fs_1", "tp"))
    in_specs = (
        P(FS_TP, None),
        P(FS, "tp"),
        P(FS, "tp"),
        P(FS, "tp"),
        P(FS, "tp"),
        P(None, "tp"),
        P("tp"),
        P(FS, "tp"),
    )
    out_specs = (P(FS_TP, None), P(FS, "tp"), P(FS, "tp"), P(None, "tp"), P("tp"))
    return jax.shard_map(
        on_device, mesh=finer, in_specs=in_specs, out_specs=out_specs, check_vma=False
    )
```

profile of v0, /device:TPU:8, one launch (start us, length us, event | category | flops | bytes accessed | tf_op | source)
XLA Modules:
  0.0 376.6 jit_solution(886776564580868433)
XLA Ops:
  7.3 0.7 all-gather.5.cloned.1.call-update
  8.0 1.8 pad_maximum_fusion.1
  9.9 1.8 convert_element_type.30
  11.8 6.5 %multiply_reduce_fusion.2 = (f32[704]{0:T(1024)S(1)}, f32[704]{0:T(1024)S(1)}, f32[704]{0:T(1024)S(1)}, f32[704]{0:T(1024)S(1)}, f32[1024,704]{0,1:T(8,128)S(1)}, /*index=5*/f32[1024,704]{0,1:T(8,128)}) fusion(f32[1024,704]{0,1:T(8,128)S(1)} %convert_element_type.30, bf16[1024,704]{0,1:T(8,128)(2,1)S(1)} %copy-done, bf16[1024,704]{0,1:T(8,128)(2,1)S(1)} %copy-done.2, ...), kind=kLoop, calls=%fused_computation.31 | loop fusion | flops 25949440 | bytes 12998656 | tf_op jit(solution)/shard_map/reduce_sum | solution.py:87
  18.3 3.0 fusion.8
  21.3 25.0 %all-gather.5.cloned.1.call-done = bf16[1024,2048]{1,0:T(8,128)(2,1)} async-done(((bf16[128,2048]{1,0:T(8,128)(2,1)}), bf16[1024,2048]{1,0:T(8,128)(2,1)}) %all-gather.5.cloned.1.call-update) | async-done | bytes 4194320 | tf_op jit(solution)/shard_map/all_gather | solution.py:94
  46.4 5.9 %fusion.3 = bf16[2048,704]{0,1:T(8,128)(2,1)S(1)} fusion(bf16[1024,704]{0,1:T(8,128)(2,1)} %fusion.8, bf16[1024,2048]{1,0:T(8,128)(2,1)} %all-gather.5.cloned.1.call-done), kind=kOutput, calls=%fused_computation.15 | convolution fusion | flops 2954231808 | bytes 8519680 | tf_op jit(solution)/shard_map/dot_general | solution.py:50
  52.3 3.9 %fusion.4 = bf16[2048,704]{0,1:T(8,128)(2,1)S(1)} fusion(bf16[1024,2048]{1,0:T(8,128)(2,1)S(1)} %copy-done.10, bf16[1024,704]{0,1:T(8,128)(2,1)S(1)} %copy-done.4, f32[1024,704]{0,1:T(8,128)S(1)} %copy-done.1), kind=kOutput, calls=%fused_computation.16 | convolution fusion | flops 2962161664 | bytes 11403264 | tf_op jit(solution)/shard_map/dot_general | solution.py:50
  56.2 3.1 pad_maximum_fusion
  59.4 8.4 %copy.22 = bf16[2048,1408]{1,0:T(8,128)(2,1)} copy(bf16[2048,1408]{0,1:T(8,128)(2,1)} %pad_maximum_fusion) | data formatting | bytes 11534336
  67.8 0.8 broadcast_in_dim.2
  68.6 10.0 %all-to-all-start.1 = ((f32[32,4,704]{2,1,0:T(4,128)}), f32[32,4,704]{2,1,0:T(4,128)S(1)}, u32[]{:S(2)}, u32[]{:S(2)}) async-start(f32[32,4,704]{2,1,0:T(4,128)} %broadcast_in_dim.2), calls=%async_computation.1 | async-start | bytes 786432 | tf_op jit(solution)/shard_map/all_to_all | solution.py:13
  78.7 60.2 %all-gather.3.cloned.1.call-done = bf16[2048,1408]{1,0:T(8,128)(2,1)} async-done(((bf16[64,1408]{1,0:T(8,128)(2,1)}), bf16[2048,1408]{1,0:T(8,128)(2,1)}) %all-gather.3.cloned.1.call-update) | async-done | bytes 5767184 | tf_op jit(solution)/shard_map/all_gather | solution.py:28
  138.9 6.0 %fusion.1 = f32[1024,2048]{1,0:T(8,128)S(1)} fusion(bf16[1024,704]{0,1:T(8,128)(2,1)} %fusion.8, bf16[2048,1408]{1,0:T(8,128)(2,1)} %all-gather.3.cloned.1.call-done), kind=kOutput, calls=%fused_computation.13 | convolution fusion | flops 2952790016 | bytes 12976128 | tf_op jit(solution)/shard_map/dot_general | solution.py:56
  144.9 7.6 %add_convert_fusion = bf16[1024,2048]{1,0:T(8,128)(2,1)} fusion(f32[1024,2048]{1,0:T(8,128)S(1)} %fusion.1, bf16[2048,1408]{1,0:T(8,128)(2,1)S(1)} %copy-done.9, bf16[1024,704]{0,1:T(8,128)(2,1)S(1)} %copy-done.5, f32[1024,704]{0,1:T(8,128)S(1)} %copy-done.1), kind=kOutput, calls=%fused_computation | convolution fusion | flops 2964914176 | bytes 20054016 | tf_op jit(solution)/shard_map/dot_general | solution.py:56
  152.5 5.0 %all-to-all-start = ((bf16[8,128,2048]{2,1,0:T(8,128)(2,1)}), bf16[8,128,2048]{2,1,0:T(8,128)(2,1)}, u32[]{:S(2)}, u32[]{:S(2)}) async-start(bf16[8,128,2048]{2,1,0:T(8,128)(2,1)} %bitcast.11), calls=%async_computation | async-start | bytes 8388608 | tf_op jit(solution)/shard_map/all_to_all | solution.py:45
  157.4 0.1 reduce_sum.62
  157.5 0.6 slice_reduce_fusion
  158.1 47.6 %all-to-all-done = bf16[8,128,2048]{2,1,0:T(8,128)(2,1)} async-done(((bf16[8,128,2048]{2,1,0:T(8,128)(2,1)}), bf16[8,128,2048]{2,1,0:T(8,128)(2,1)}, u32[]{:S(2)}, u32[]{:S(2)}) %all-to-all-start) | async-done | bytes 4194336 | tf_op jit(solution)/shard_map/all_to_all | solution.py:45
  205.8 4.0 %reduce_sum.57 = bf16[128,2048]{1,0:T(8,128)(2,1)} reduce(bf16[8,128,2048]{2,1,0:T(8,128)(2,1)} %all-to-all-done, bf16[]{:T(256)} %constant.19.clone.1), dimensions={0}, to_apply=%region_0.1 | reduce | flops 1835008 | bytes 4718594 | tf_op jit(solution)/shard_map/reduce_sum | solution.py:46
  209.7 157.4 %reduce-scatter.4.cloned.1.call-done = bf16[64,1408]{1,0:T(8,128)(2,1)} async-done(((bf16[2048,1408]{1,0:T(8,128)(2,1)}), bf16[64,1408]{1,0:T(8,128)(2,1)}) %reduce-scatter.4.cloned.1.call-update) | async-done | bytes 180240
  367.2 1.1 copy.23
  368.4 0.8 copy.21
  369.3 0.8 copy.20
  (37 shorter events, 0.4 us)
Async XLA Ops:
  7.2 4.6 %copy-start = (bf16[1024,704]{0,1:T(8,128)(2,1)S(1)}, bf16[1024,704]{0,1:T(8,128)(2,1)}, u32[]{:S(2)}) copy-start(bf16[1024,704]{0,1:T(8,128)(2,1)} %param.9) | copy-start | bytes 4325380
  7.2 4.5 %copy-start.7 = (f32[3,704]{1,0:T(4,128)S(1)}, f32[3,704]{1,0:T(4,128)}, u32[]{:S(2)}) copy-start(f32[3,704]{1,0:T(4,128)} %param.13) | copy-start | bytes 25348
  7.2 4.6 %copy-start.8 = (f32[704]{0:T(1024)S(1)}, f32[704]{0:T(1024)}, u32[]{:S(2)}) copy-start(f32[704]{0:T(1024)} %param.14) | copy-start | bytes 8452
  7.2 4.6 %copy-start.2 = (bf16[1024,704]{0,1:T(8,128)(2,1)S(1)}, bf16[1024,704]{0,1:T(8,128)(2,1)}, u32[]{:S(2)}) copy-start(bf16[1024,704]{0,1:T(8,128)(2,1)} %param.10) | copy-start | bytes 4325380
  7.2 39.2 %all-gather.5.cloned.1.call-start = ((), (), s32[]{:S(2)}) async-start(), calls=%async_computation.4 | async-start | bytes 4718592 | tf_op jit(solution)/shard_map/all_gather | solution.py:94
  7.9 131.0 %all-gather.3.cloned.1.call-start = ((), (), s32[]{:S(2)}) async-start(), calls=%async_computation.3 | async-start | bytes 5947392 | tf_op jit(solution)/shard_map/all_gather | solution.py:28
  9.8 357.4 %reduce-scatter.4.cloned.1.call-start = ((), (), s32[]{:S(2)}) async-start(), calls=%async_computation.5 | async-start | bytes 5947392
  9.9 1.9 copy-start.3
  21.3 31.0 %copy-start.1 = (f32[1024,704]{0,1:T(8,128)S(1)}, f32[1024,704]{0,1:T(8,128)}, u32[]{:S(2)}) copy-start(f32[1024,704]{0,1:T(8,128)} %get-tuple-element.33) | copy-start | bytes 8650756
  46.4 5.9 %copy-start.4 = (bf16[1024,704]{0,1:T(8,128)(2,1)S(1)}, bf16[1024,704]{0,1:T(8,128)(2,1)}, u32[]{:S(2)}) copy-start(bf16[1024,704]{0,1:T(8,128)(2,1)} %param.15) | copy-start | bytes 4325380
  46.4 5.9 %copy-start.10 = (bf16[1024,2048]{1,0:T(8,128)(2,1)S(1)}, bf16[1024,2048]{1,0:T(8,128)(2,1)}, u32[]{:S(2)}) copy-start(bf16[1024,2048]{1,0:T(8,128)(2,1)} %all-gather.5.cloned.1.call-done) | copy-start | bytes 12582916
  68.6 83.8 %all-to-all-start.1 = ((f32[32,4,704]{2,1,0:T(4,128)}), f32[32,4,704]{2,1,0:T(4,128)S(1)}, u32[]{:S(2)}, u32[]{:S(2)}) async-start(f32[32,4,704]{2,1,0:T(4,128)} %broadcast_in_dim.2), calls=%async_computation.1 | async-start | bytes 786432 | tf_op jit(solution)/shard_map/all_to_all | solution.py:13
  138.9 6.0 %copy-start.5 = (bf16[1024,704]{0,1:T(8,128)(2,1)S(1)}, bf16[1024,704]{0,1:T(8,128)(2,1)}, u32[]{:S(2)}) copy-start(bf16[1024,704]{0,1:T(8,128)(2,1)} %param.15) | copy-start | bytes 4325380
  138.9 6.0 %copy-start.9 = (bf16[2048,1408]{1,0:T(8,128)(2,1)S(1)}, bf16[2048,1408]{1,0:T(8,128)(2,1)}, u32[]{:S(2)}) copy-start(bf16[2048,1408]{1,0:T(8,128)(2,1)} %all-gather.3.cloned.1.call-done) | copy-start | bytes 17301508
  152.5 53.3 %all-to-all-start = ((bf16[8,128,2048]{2,1,0:T(8,128)(2,1)}), bf16[8,128,2048]{2,1,0:T(8,128)(2,1)}, u32[]{:S(2)}, u32[]{:S(2)}) async-start(bf16[8,128,2048]{2,1,0:T(8,128)(2,1)} %bitcast.11), calls=%async_computation | async-start | bytes 8388608 | tf_op jit(solution)/shard_map/all_to_all | solution.py:45
  157.5 210.8 %copy-start.6 = (f32[4,704]{1,0:T(4,128)}, f32[4,704]{1,0:T(4,128)S(1)}, u32[]{:S(2)}) copy-start(f32[4,704]{1,0:T(4,128)S(1)} %broadcast_multiply_fusion) | copy-start | bytes 33796
Sparse Core Ops, SparseCore 0:
  9.9 36.4 all-gather.4
  49.5 89.3 all-gather.2
  142.9 224.2 reduce-scatter.3
where the time goes:
time: 377 us
  waiting for transfers between devices  291 us (77%)
  matrix products  23.3 us (6%)
  other arithmetic  20.5 us (5%)
  starting transfers between devices  15.1 us (4%)
  between operations  14 us (4%)
  local copies, waits for them, and re-layouts  12.7 us (3%)
    unnamed x4, waiting for transfers between devices  158 us
    all_gather x1, waiting for transfers between devices, in_one_piece(): lax.all_gather(both, axis, axis=dim, tiled=True)  60.2 us
    all_to_all x1, waiting for transfers between devices, summed_on_arrival(): lax.all_to_all(blocks, axis, split_axis=0, concat_axis=0, tiled=True)  47.6 us
    all_gather x1, waiting for transfers between devices, on_device(): whole_tokens = lax.all_gather(tokens, 'tp', axis=0, tiled=True)  25 us
    dot_general x2, matrix products, contract_cols(): lax.dot_general(left, right, (((1,), (1,)), ((), ())), preferred_element_...  13.5 us
    unnamed x26, local copies, waits for them, and re-layouts  11.2 us
    all_to_all x1, starting transfers between devices, copy_for_each(): lax.all_to_all(jnp.broadcast_to(shard[None], (peers, *shard.shape)), axis...  10 us
    dot_general x2, matrix products, contract_rows(): lax.dot_general(left, right, (((0,), (0,)), ((), ())), preferred_element_...  9.78 us
  transfers between devices with their start and end apart: 5, of which 4 were waited for; matrix products, arithmetic and copies ran while one was open for 14% of the time, Pallas kernels for 0%

commit v1 on v0

--- a/solution.py
+++ b/solution.py
@@ -91,7 +91,22 @@
         ]
     )
     conv_total = taken_together(conv_terms, FS) * scale
-    whole_tokens = lax.all_gather(tokens, "tp", axis=0, tiled=True)
+    ways, here, step = (lax.axis_size("tp"), lax.axis_index("tp"), tokens.shape[0])
+    shape = [n * ways if d == 0 else n for d, n in enumerate(tokens.shape)]
+    whole_tokens = lax.dynamic_update_slice_in_dim(
+        jnp.zeros(shape, tokens.dtype), tokens, here * step, axis=0
+    )
+    going_up = going_down = tokens
+    for far in range(1, ways // 2 + 1):
+        going_up = lax.ppermute(going_up, "tp", [(d, (d + 1) % ways) for d in range(ways)])
+        whole_tokens = lax.dynamic_update_slice_in_dim(
+            whole_tokens, going_up, (here - far) % ways * step, axis=0
+        )
+        if 2 * far < ways:
+            going_down = lax.ppermute(going_down, "tp", [(d, (d - 1) % ways) for d in range(ways)])
+            whole_tokens = lax.dynamic_update_slice_in_dim(
+                whole_tokens, going_down, (here + far) % ways * step, axis=0
+            )
     full_gate, full_value = in_one_piece((up_gate_w, up_value_w), FS, 0, 1)
     joined = summed_rows(
         jnp.concatenate(

time: 377 us -> 352 us (0.934)
  waiting for transfers between devices: 291 us -> 245 us
  local copies, waits for them, and re-layouts: 12.7 us -> 24 us
  starting transfers between devices: 15.1 us -> 21.9 us
    unnamed x4 -> x3, waiting for transfers between devices: 158 us -> 210 us
    all_to_all x1, waiting for transfers between devices: 47.6 us -> 0.01 us  [summed_on_arrival(): lax.all_to_all(blocks, axis, split_axis=0, concat_axis=0, tiled=True)]
    all_gather x1, waiting for transfers between devices: 60.2 us -> 26.6 us  [in_one_piece(): lax.all_gather(both, axis, axis=dim, tiled=True)]
    all_gather x1 -> x0, waiting for transfers between devices: 25 us -> none  [on_device(): whole_tokens = lax.all_gather(tokens, 'tp', axis=0, tiled=True)]
    ppermute x0 -> x7, waiting for transfers between devices: none -> 9.28 us  [the longest x4 8.56 us: on_device(): lax.ppermute(going_up, 'tp', [(d, (d + 1) % ways) for d in range(ways)])]
    dynamic_update_slice x0 -> x8, local copies, waits for them, and re-layouts: none -> 8.95 us  [the longest x4 5.54 us: on_device(): lax.dynamic_update_slice_in_dim(whole_tokens, going_up, (here - far) % wa...]
    ppermute x0 -> x7, starting transfers between devices: none -> 5.27 us  [the longest x3 5.24 us: on_device(): lax.ppermute(going_down, 'tp', [(d, (d - 1) % ways) for d in range(ways)])]
    unnamed x26 -> x28, local copies, waits for them, and re-layouts: 11.2 us -> 11.1 us
  transfers between devices with their start and end apart: 5 -> 11, of which waited for: 4 -> 6; matrix products, arithmetic and copies ran while one was open for 14% -> 18% of each run, Pallas kernels for 0% -> 0%
where the time goes in v1:
time: 352 us; the launch traced here: 351 us
  waiting for transfers between devices  245 us (70%)
  matrix products  25.3 us (7%)
  local copies, waits for them, and re-layouts  24 us (7%)
  starting transfers between devices  21.9 us (6%)
  other arithmetic  20.2 us (6%)
  between operations  14.3 us (4%)
    unnamed x3, waiting for transfers between devices  210 us
    all_gather x1, waiting for transfers between devices, in_one_piece(): lax.all_gather(both, axis, axis=dim, tiled=True)  26.6 us
    dot_general x2, matrix products, contract_cols(): lax.dot_general(left, right, (((1,), (1,)), ((), ())), preferred_element_...  13.5 us
    dot_general x2, matrix products, contract_rows(): lax.dot_general(left, right, (((0,), (0,)), ((), ())), preferred_element_...  11.7 us
    all_to_all x1, starting transfers between devices, copy_for_each(): lax.all_to_all(jnp.broadcast_to(shard[None], (peers, *shard.shape)), axis...  11.6 us
    unnamed x28, local copies, waits for them, and re-layouts  11.1 us
    ppermute x4, waiting for transfers between devices, on_device(): lax.ppermute(going_up, 'tp', [(d, (d + 1) % ways) for d in range(ways)])  8.56 us
  transfers between devices with their start and end apart: 11, of which 6 were waited for; matrix products, arithmetic and copies ran while one was open for 18% of the time, Pallas kernels for 0%

profile of v1, /device:TPU:8, one launch (start us, length us, event | category | flops | bytes accessed | tf_op | source)
XLA Modules:
  0.0 351.1 jit_solution(15994006144743202194)
XLA Ops:
  7.2 1.7 pad_maximum_fusion.1
  9.1 1.7 collective-permute-start.1
  10.8 1.7 convert_element_type.30
  12.6 6.5 %multiply_reduce_fusion.2 = (f32[704]{0:T(1024)S(1)}, f32[704]{0:T(1024)S(1)}, f32[704]{0:T(1024)S(1)}, f32[704]{0:T(1024)S(1)}, f32[1024,704]{0,1:T(8,128)S(1)}, /*index=5*/f32[1024,704]{0,1:T(8,128)}) fusion(f32[1024,704]{0,1:T(8,128)S(1)} %convert_element_type.30, bf16[1024,704]{0,1:T(8,128)(2,1)S(1)} %copy-done, bf16[1024,704]{0,1:T(8,128)(2,1)S(1)} %copy-done.2, ...), kind=kLoop, calls=%fused_computation.29 | loop fusion | flops 25949440 | bytes 12998656 | tf_op jit(solution)/shard_map/reduce_sum | solution.py:87
  19.2 3.0 fusion.6
  22.1 1.7 collective-permute-start.3
  23.9 2.5 broadcast_in_dim.4
  28.1 1.9 constant_dynamic-update-slice_fusion.6
  30.8 1.8 collective-permute-start.5
  32.6 1.9 constant_dynamic-update-slice_fusion.4
  34.5 2.4 collective-permute-done.4
  40.2 5.3 %collective-permute-done.6 = bf16[128,2048]{1,0:T(8,128)(2,1)S(1)} collective-permute-done((bf16[128,2048]{1,0:T(8,128)(2,1)S(1)}, bf16[128,2048]{1,0:T(8,128)(2,1)S(1)}, u32[]{:S(2)}, u32[]{:S(2)}) %collective-permute-start.6) | collective-permute-done | bytes 524320 | tf_op jit(solution)/shard_map/ppermute | solution.py:101
  46.4 5.7 %convolution_convert_fusion.1 = bf16[2048,704]{0,1:T(8,128)(2,1)S(1)} fusion(bf16[1024,704]{0,1:T(8,128)(2,1)S(1)} %copy-done.6, bf16[1024,2048]{1,0:T(8,128)(2,1)} %constant_dynamic-update-slice_fusion), kind=kOutput, calls=%fused_computation.7 | convolution fusion | flops 2954231808 | bytes 8519680 | tf_op jit(solution)/shard_map/dot_general | solution.py:50
  52.2 6.0 %convolution_convert_fusion = bf16[2048,704]{0,1:T(8,128)(2,1)S(1)} fusion(bf16[1024,2048]{1,0:T(8,128)(2,1)} %constant_dynamic-update-slice_fusion, bf16[1024,704]{0,1:T(8,128)(2,1)S(1)} %copy-done.4, f32[1024,704]{0,1:T(8,128)S(1)} %copy-done.1), kind=kOutput, calls=%fused_computation.6 | convolution fusion | flops 2962161664 | bytes 11403264 | tf_op jit(solution)/shard_map/dot_general | solution.py:50
  58.2 3.1 pad_maximum_fusion
  61.4 8.3 %copy.22 = bf16[2048,1408]{1,0:T(8,128)(2,1)} copy(bf16[2048,1408]{0,1:T(8,128)(2,1)} %pad_maximum_fusion) | data formatting | bytes 11534336
  70.5 11.6 %all-to-all-start.1 = ((f32[32,4,704]{2,1,0:T(4,128)}), f32[32,4,704]{2,1,0:T(4,128)S(1)}, u32[]{:S(2)}, u32[]{:S(2)}) async-start(f32[32,4,704]{2,1,0:T(4,128)} %broadcast_in_dim.5), calls=%async_computation.1 | async-start | bytes 786432 | tf_op jit(solution)/shard_map/all_to_all | solution.py:13
  82.2 26.6 %all-gather.2.cloned.1.call-done = bf16[2048,1408]{1,0:T(8,128)(2,1)} async-done(((bf16[64,1408]{1,0:T(8,128)(2,1)}), bf16[2048,1408]{1,0:T(8,128)(2,1)}) %all-gather.2.cloned.1.call-update) | async-done | bytes 5767184 | tf_op jit(solution)/shard_map/all_gather | solution.py:28
  108.7 6.0 %fusion.1 = f32[1024,2048]{1,0:T(8,128)S(1)} fusion(bf16[1024,704]{0,1:T(8,128)(2,1)} %fusion.6, bf16[2048,1408]{1,0:T(8,128)(2,1)} %all-gather.2.cloned.1.call-done), kind=kOutput, calls=%fused_computation.13 | convolution fusion | flops 2952790016 | bytes 12976128 | tf_op jit(solution)/shard_map/dot_general | solution.py:56
  114.7 7.6 %add_convert_fusion = bf16[1024,2048]{1,0:T(8,128)(2,1)} fusion(f32[1024,2048]{1,0:T(8,128)S(1)} %fusion.1, bf16[2048,1408]{1,0:T(8,128)(2,1)S(1)} %copy-done.11, bf16[1024,704]{0,1:T(8,128)(2,1)S(1)} %copy-done.5, f32[1024,704]{0,1:T(8,128)S(1)} %copy-done.1), kind=kOutput, calls=%fused_computation | convolution fusion | flops 2964914176 | bytes 20054016 | tf_op jit(solution)/shard_map/dot_general | solution.py:56
  122.3 4.9 %all-to-all-start = ((bf16[8,128,2048]{2,1,0:T(8,128)(2,1)}), bf16[8,128,2048]{2,1,0:T(8,128)(2,1)}, u32[]{:S(2)}, u32[]{:S(2)}) async-start(bf16[8,128,2048]{2,1,0:T(8,128)(2,1)} %bitcast.7), calls=%async_computation | async-start | bytes 8388608 | tf_op jit(solution)/shard_map/all_to_all | solution.py:45
  127.9 209.5 %reduce-scatter.4.cloned.1.call-done = bf16[64,1408]{1,0:T(8,128)(2,1)} async-done(((bf16[2048,1408]{1,0:T(8,128)(2,1)}), bf16[64,1408]{1,0:T(8,128)(2,1)}) %reduce-scatter.4.cloned.1.call-update) | async-done | bytes 180240
  337.4 1.1 copy.23
  340.4 3.8 %reduce_sum.57 = bf16[128,2048]{1,0:T(8,128)(2,1)} reduce(bf16[8,128,2048]{2,1,0:T(8,128)(2,1)} %all-to-all-done, bf16[]{:T(256)} %constant.67.clone.1), dimensions={0}, to_apply=%region_0.1 | reduce | flops 1835008 | bytes 4718594 | tf_op jit(solution)/shard_map/reduce_sum | solution.py:46
  (59 shorter events, 10.2 us)
Async XLA Ops:
  7.2 5.4 %copy-start.9 = (f32[3,704]{1,0:T(4,128)S(1)}, f32[3,704]{1,0:T(4,128)}, u32[]{:S(2)}) copy-start(f32[3,704]{1,0:T(4,128)} %param.13) | copy-start | bytes 25348
  7.2 5.4 %copy-start.10 = (f32[704]{0:T(1024)S(1)}, f32[704]{0:T(1024)}, u32[]{:S(2)}) copy-start(f32[704]{0:T(1024)} %param.14) | copy-start | bytes 8452
  7.2 101.5 %all-gather.2.cloned.1.call-start = ((), (), s32[]{:S(2)}) async-start(), calls=%async_computation.3 | async-start | bytes 5947392 | tf_op jit(solution)/shard_map/all_gather | solution.py:28
  9.0 328.5 %reduce-scatter.4.cloned.1.call-start = ((), (), s32[]{:S(2)}) async-start(), calls=%async_computation.4 | async-start | bytes 5947392
  9.0 3.6 %copy-start = (bf16[1024,704]{0,1:T(8,128)(2,1)S(1)}, bf16[1024,704]{0,1:T(8,128)(2,1)}, u32[]{:S(2)}) copy-start(bf16[1024,704]{0,1:T(8,128)(2,1)} %param.9) | copy-start | bytes 4325380
  9.0 3.6 %copy-start.2 = (bf16[1024,704]{0,1:T(8,128)(2,1)S(1)}, bf16[1024,704]{0,1:T(8,128)(2,1)}, u32[]{:S(2)}) copy-start(bf16[1024,704]{0,1:T(8,128)(2,1)} %param.10) | copy-start | bytes 4325380
  9.0 3.6 %copy-start.3 = (bf16[1024,704]{0,1:T(8,128)(2,1)S(1)}, bf16[1024,704]{0,1:T(8,128)(2,1)}, u32[]{:S(2)}) copy-start(bf16[1024,704]{0,1:T(8,128)(2,1)} %param.15) | copy-start | bytes 4325380
  9.1 10.1 %collective-permute-start = (bf16[128,2048]{1,0:T(8,128)(2,1)}, bf16[128,2048]{1,0:T(8,128)(2,1)}, u32[]{:S(2)}, u32[]{:S(2)}) collective-permute-start(bf16[128,2048]{1,0:T(8,128)(2,1)} %param.8), channel_id=1, source_target_pairs={{0,1},{1,2},{2,3},{3,4},{4,5},{5,6},{6,7},{7,0},{8,9},{9,10},{10,1... | collective-permute-start | bytes 1572872 | tf_op jit(solution)/shard_map/ppermute | solution.py:101
  9.1 13.1 %collective-permute-start.1 = (bf16[128,2048]{1,0:T(8,128)(2,1)}, bf16[128,2048]{1,0:T(8,128)(2,1)S(1)}, u32[]{:S(2)}, u32[]{:S(2)}) collective-permute-start(bf16[128,2048]{1,0:T(8,128)(2,1)} %param.8), channel_id=1, source_target_pairs={{0,7},{1,0},{2,1},{3,2},{4,3},{5,4},{6,5},{7,6},{8,15},{9,8},{10,9... | collective-permute-start | bytes 1572872 | tf_op jit(solution)/shard_map/ppermute | solution.py:106
  19.2 8.9 %collective-permute-start.2 = (bf16[128,2048]{1,0:T(8,128)(2,1)}, bf16[128,2048]{1,0:T(8,128)(2,1)}, u32[]{:S(2)}, u32[]{:S(2)}) collective-permute-start(bf16[128,2048]{1,0:T(8,128)(2,1)} %collective-permute-done), channel_id=1, source_target_pairs={{0,1},{1,2},{2,3},{3,4},{4,5},{5,6},{6,7},{7,0},{8,9},{9,10},{10,1... | collective-permute-start | bytes 1572872 | tf_op jit(solution)/shard_map/ppermute | solution.py:101
  22.1 4.3 %copy-start.7 = (bf16[128,2048]{1,0:T(8,128)(2,1)S(1)}, bf16[128,2048]{1,0:T(8,128)(2,1)}, u32[]{:S(2)}) copy-start(bf16[128,2048]{1,0:T(8,128)(2,1)} %param.8) | copy-start | bytes 1572868
  22.1 8.7 %collective-permute-start.3 = (bf16[128,2048]{1,0:T(8,128)(2,1)S(1)}, bf16[128,2048]{1,0:T(8,128)(2,1)S(1)}, u32[]{:S(2)}, u32[]{:S(2)}) collective-permute-start(bf16[128,2048]{1,0:T(8,128)(2,1)S(1)} %collective-permute-done.1), channel_id=1, source_target_pairs={{0,7},{1,0},{2,1},{3,2},{4,3},{5,4},{6,5},{7,6},{8,15},{9,8},{10,9... | collective-permute-start | bytes 1572872 | tf_op jit(solution)/shard_map/ppermute | solution.py:106
  28.1 8.8 %collective-permute-start.4 = (bf16[128,2048]{1,0:T(8,128)(2,1)}, bf16[128,2048]{1,0:T(8,128)(2,1)S(1)}, u32[]{:S(2)}, u32[]{:S(2)}) collective-permute-start(bf16[128,2048]{1,0:T(8,128)(2,1)} %collective-permute-done.2), channel_id=1, source_target_pairs={{0,1},{1,2},{2,3},{3,4},{4,5},{5,6},{6,7},{7,0},{8,9},{9,10},{10,1... | collective-permute-start | bytes 1572872 | tf_op jit(solution)/shard_map/ppermute | solution.py:101
  30.8 15.6 %copy-start.6 = (bf16[1024,704]{0,1:T(8,128)(2,1)S(1)}, bf16[1024,704]{0,1:T(8,128)(2,1)}, u32[]{:S(2)}) copy-start(bf16[1024,704]{0,1:T(8,128)(2,1)} %fusion.6) | copy-start | bytes 4325380
  30.8 8.5 %collective-permute-start.5 = (bf16[128,2048]{1,0:T(8,128)(2,1)S(1)}, bf16[128,2048]{1,0:T(8,128)(2,1)S(1)}, u32[]{:S(2)}, u32[]{:S(2)}) collective-permute-start(bf16[128,2048]{1,0:T(8,128)(2,1)S(1)} %collective-permute-done.3), channel_id=1, source_target_pairs={{0,7},{1,0},{2,1},{3,2},{4,3},{5,4},{6,5},{7,6},{8,15},{9,8},{10,9... | collective-permute-start | bytes 1572872 | tf_op jit(solution)/shard_map/ppermute | solution.py:106
  36.9 8.6 %collective-permute-start.6 = (bf16[128,2048]{1,0:T(8,128)(2,1)S(1)}, bf16[128,2048]{1,0:T(8,128)(2,1)S(1)}, u32[]{:S(2)}, u32[]{:S(2)}) collective-permute-start(bf16[128,2048]{1,0:T(8,128)(2,1)S(1)} %collective-permute-done.4), channel_id=1, source_target_pairs={{0,1},{1,2},{2,3},{3,4},{4,5},{5,6},{6,7},{7,0},{8,9},{9,10},{10,1... | collective-permute-start | bytes 1572872 | tf_op jit(solution)/shard_map/ppermute | solution.py:101
  46.4 5.8 %copy-start.1 = (f32[1024,704]{0,1:T(8,128)S(1)}, f32[1024,704]{0,1:T(8,128)}, u32[]{:S(2)}) copy-start(f32[1024,704]{0,1:T(8,128)} %get-tuple-element.33) | copy-start | bytes 8650756
  46.4 5.8 %copy-start.4 = (bf16[1024,704]{0,1:T(8,128)(2,1)S(1)}, bf16[1024,704]{0,1:T(8,128)(2,1)}, u32[]{:S(2)}) copy-start(bf16[1024,704]{0,1:T(8,128)(2,1)} %param.15) | copy-start | bytes 4325380
  70.5 51.8 %all-to-all-start.1 = ((f32[32,4,704]{2,1,0:T(4,128)}), f32[32,4,704]{2,1,0:T(4,128)S(1)}, u32[]{:S(2)}, u32[]{:S(2)}) async-start(f32[32,4,704]{2,1,0:T(4,128)} %broadcast_in_dim.5), calls=%async_computation.1 | async-start | bytes 786432 | tf_op jit(solution)/shard_map/all_to_all | solution.py:13
  108.7 6.0 %copy-start.5 = (bf16[1024,704]{0,1:T(8,128)(2,1)S(1)}, bf16[1024,704]{0,1:T(8,128)(2,1)}, u32[]{:S(2)}) copy-start(bf16[1024,704]{0,1:T(8,128)(2,1)} %param.15) | copy-start | bytes 4325380
  108.7 6.0 %copy-start.11 = (bf16[2048,1408]{1,0:T(8,128)(2,1)S(1)}, bf16[2048,1408]{1,0:T(8,128)(2,1)}, u32[]{:S(2)}) copy-start(bf16[2048,1408]{1,0:T(8,128)(2,1)} %all-gather.2.cloned.1.call-done) | copy-start | bytes 17301508
  122.3 218.1 %all-to-all-start = ((bf16[8,128,2048]{2,1,0:T(8,128)(2,1)}), bf16[8,128,2048]{2,1,0:T(8,128)(2,1)}, u32[]{:S(2)}, u32[]{:S(2)}) async-start(bf16[8,128,2048]{2,1,0:T(8,128)(2,1)} %bitcast.7), calls=%async_computation | async-start | bytes 8388608 | tf_op jit(solution)/shard_map/all_to_all | solution.py:45
  127.3 216.9 %copy-start.8 = (f32[4,704]{1,0:T(4,128)}, f32[4,704]{1,0:T(4,128)S(1)}, u32[]{:S(2)}) copy-start(f32[4,704]{1,0:T(4,128)S(1)} %broadcast_multiply_fusion) | copy-start | bytes 33796
Sparse Core Ops, SparseCore 0:
  11.1 97.5 all-gather.1
  112.7 224.7 reduce-scatter.3
